TPU v7x, 32 devices: a whole 2x2x4 slice. The times are simulated.
32 devices in a mesh: rep: 2 (over x), fs: 8 (over z, y), tp: 2 (over core).
Axes of the slice: x: 2, y: 2, z: 4, core: 2. Of those that a mesh axis runs over, the one named last changes fastest.
Arguments:
- tokens: bfloat16 [6144, 2048], P(('rep', 'fs'), 'tp'), may hold values from -6 to 6
- mixing_norm_gain: float32 [2048], replicated, may hold values from 0.1 to 1.9
- recurrent_input_weight: float32 [2048, 3072], P('fs', 'tp'), may hold values from -0.125 to 0.125
- recurrent_input_scale: float32 [3072], P('tp'), may hold values from 0.5 to 2
- convolution_kernel_taps: float32 [4, 3072], P(None, 'tp'), may hold values from -3 to 3
- recurrence_gate_weight_blocks: bfloat16 [24, 128, 128], P('tp'), may hold values from -0.5 to 0.5
- input_gate_weight_blocks: bfloat16 [24, 128, 128], P('tp'), may hold values from -0.5 to 0.5
- channel_decay_parameter: float32 [3072], P('tp'), may hold values from 3 to 9
- token_extra_log_decay: float32 [6144], P(('rep', 'fs')), may hold values from -0.7 to 0
- mixing_output_weight: float32 [3072, 2048], P('tp', 'fs'), may hold values from -0.109375 to 0.109375
- mixing_output_scale: float32 [2048], P('fs'), may hold values from 0.5 to 2
- feedforward_norm_gain: float32 [2048], replicated, may hold values from 0.1 to 1.9
- feedforward_gate_weight: float32 [2048, 5120], P('fs', 'tp'), may hold values from -0.125 to 0.125
- feedforward_gate_scale: float32 [5120], P('tp'), may hold values from 0.5 to 2
- feedforward_up_weight: float32 [2048, 5120], P('fs', 'tp'), may hold values from -0.125 to 0.125
- feedforward_up_scale: float32 [5120], P('tp'), may hold values from 0.5 to 2
- feedforward_down_weight: float32 [5120, 2048], P('tp', 'fs'), may hold values from -0.078125 to 0.078125
- feedforward_down_scale: float32 [2048], P('fs'), may hold values from 0.5 to 2
Outputs:
- layer_out: bfloat16 [6144, 2048], P(('rep', 'fs'), 'tp')
All inputs are finite; a program needn't handle non-finite values.
Results may differ from a plain program's by a relative error of at most 0.02.
Values may be sent and summed in bfloat16 or wider, within the bound.
A program may use at most 128 MiB of HBM per device.

v0:
```python
import jax
import jax.numpy as jnp
from jax import lax
from jax.sharding import PartitionSpec as P

EPS = 1e-06
DECAY_FACTOR = 8.0


def row_norm(rows, gain_vec):
    values = rows.astype(jnp.float32)
    inverse = lax.rsqrt(jnp.mean(values * values, axis=-1, keepdims=True) + EPS)
    return (values * inverse * gain_vec).astype(jnp.bfloat16)


def gather_normed(rows, gain_vec):
    whole_rows = lax.all_gather(rows, "tp", axis=1, tiled=True)
    return row_norm(whole_rows, gain_vec)


def share_sums(terms):
    return lax.psum_scatter(
        terms.astype(jnp.bfloat16), "tp", scatter_dimension=1, tiled=True
    ).astype(jnp.float32)


def combine_pairs(earlier, later):
    decay_one, value_one = earlier
    decay_two, value_two = later
    return (decay_one * decay_two, decay_two * value_one + value_two)


def add_one(left_rows, weight_piece):
    return jnp.dot(left_rows, weight_piece, preferred_element_type=jnp.float32)


def place_columns(left_rows, total_now, pieces, start_row):
    weight_piece, scale_piece = pieces
    product = jnp.dot(left_rows, weight_piece, preferred_element_type=jnp.float32) * scale_piece
    return lax.dynamic_update_slice_in_dim(total_now, product, start_row, 1)


def body(
    tokens,
    mixing_norm_gain,
    recurrent_input_weight,
    recurrent_input_scale,
    convolution_kernel_taps,
    recurrence_gate_weight_blocks,
    input_gate_weight_blocks,
    channel_decay_parameter,
    token_extra_log_decay,
    mixing_output_weight,
    mixing_output_scale,
    feedforward_norm_gain,
    feedforward_gate_weight,
    feedforward_gate_scale,
    feedforward_up_weight,
    feedforward_up_scale,
    feedforward_down_weight,
    feedforward_down_scale,
):
    normed = gather_normed(tokens, mixing_norm_gain)
    seq_rows = normed.shape[0]
    model_width = normed.shape[1]
    width_dev = recurrent_input_weight.shape[1]
    rec_sum = add_one(
        normed,
        lax.all_gather(recurrent_input_weight.astype(jnp.bfloat16), "fs", axis=0, tiled=True),
    )
    rec_input = (rec_sum * recurrent_input_scale).astype(jnp.bfloat16)
    rec_f32 = rec_input.astype(jnp.float32)
    tap_count = convolution_kernel_taps.shape[0]
    padded = jnp.pad(rec_f32, ((tap_count - 1, 0), (0, 0)))
    conv_out = jnp.zeros((seq_rows, width_dev), jnp.float32)
    for tap_index in range(tap_count):
        conv_out = (
            conv_out + convolution_kernel_taps[tap_index] * padded[tap_index : tap_index + seq_rows]
        )
    block_count = recurrence_gate_weight_blocks.shape[0]
    block_size = recurrence_gate_weight_blocks.shape[1]
    blocks = conv_out.astype(jnp.bfloat16).reshape(seq_rows, block_count, block_size)
    recurrence_gate_values = jax.nn.sigmoid(
        jnp.einsum(
            "lni,nij->lnj",
            blocks,
            recurrence_gate_weight_blocks,
            preferred_element_type=jnp.float32,
        ).reshape(seq_rows, width_dev)
    )
    input_gate = jax.nn.sigmoid(
        jnp.einsum(
            "lni,nij->lnj", blocks, input_gate_weight_blocks, preferred_element_type=jnp.float32
        ).reshape(seq_rows, width_dev)
    )
    decay_logarithm = (
        -DECAY_FACTOR * recurrence_gate_values * jax.nn.softplus(-channel_decay_parameter)
        + token_extra_log_decay[:, None]
    )
    decay = jnp.exp(decay_logarithm)
    drive = jnp.sqrt(-jnp.expm1(2.0 * decay_logarithm)) * input_gate * conv_out
    _, state = lax.associative_scan(combine_pairs, (decay, drive), axis=0)
    state_low = state.astype(jnp.bfloat16)
    mix_terms = place_columns(
        state_low,
        jnp.zeros((seq_rows, model_width), jnp.float32),
        (
            lax.all_gather(mixing_output_weight.astype(jnp.bfloat16), "fs", axis=1, tiled=True),
            lax.all_gather(
                mixing_output_scale.reshape(1, -1).astype(jnp.bfloat16), "fs", axis=1, tiled=True
            ).astype(jnp.float32),
        ),
        jnp.int32(0),
    )
    mixed = (tokens.astype(jnp.float32) + share_sums(mix_terms)).astype(jnp.bfloat16)
    normed_ffn = gather_normed(mixed, feedforward_norm_gain)
    gate_sum = add_one(
        normed_ffn,
        lax.all_gather(feedforward_gate_weight.astype(jnp.bfloat16), "fs", axis=0, tiled=True),
    )
    up_sum = add_one(
        normed_ffn,
        lax.all_gather(feedforward_up_weight.astype(jnp.bfloat16), "fs", axis=0, tiled=True),
    )
    hidden = (
        jax.nn.silu(gate_sum * feedforward_gate_scale) * (up_sum * feedforward_up_scale)
    ).astype(jnp.bfloat16)
    down_terms = place_columns(
        hidden,
        jnp.zeros((seq_rows, model_width), jnp.float32),
        (
            lax.all_gather(feedforward_down_weight.astype(jnp.bfloat16), "fs", axis=1, tiled=True),
            lax.all_gather(
                feedforward_down_scale.reshape(1, -1).astype(jnp.bfloat16), "fs", axis=1, tiled=True
            ).astype(jnp.float32),
        ),
        jnp.int32(0),
    )
    return (mixed.astype(jnp.float32) + share_sums(down_terms)).astype(jnp.bfloat16)


def solution(mesh):
    placed = (
        P(("rep", "fs"), "tp"),
        P(),
        P("fs", "tp"),
        P("tp"),
        P(None, "tp"),
        P("tp", None, None),
        P("tp", None, None),
        P("tp"),
        P(("rep", "fs")),
        P("tp", "fs"),
        P("fs"),
        P(),
        P("fs", "tp"),
        P("tp"),
        P("fs", "tp"),
        P("tp"),
        P("tp", "fs"),
        P("fs"),
    )
    return jax.shard_map(
        body, mesh=mesh, in_specs=placed, out_specs=P(("rep", "fs"), "tp"), check_vma=False
    )
```

profile of v0, /device:TPU:0, one launch (start us, length us, event | category | flops | bytes accessed | tf_op | source)
XLA Modules:
  0.0 784.1 jit_solution(13299143010067147832)
XLA Ops:
  11.0 22.3 %all-gather.2 = bf16[8,1,256]{2,1,0:T(2,128)(2,1)S(1)} all-gather(bf16[1,1,256]{2,1,0:T(2,128)(2,1)S(1)} %reshape.53), channel_id=2, replica_groups=mesh['rep'=2,'fs'=8,'tp'=2] {'fs'}, dimensions={0}, use_global_device_ids=true | all-gather | bytes 4608 | tf_op jit(solution)/shard_map/all_gather | solution.py:109
  35.8 87.7 %all-gather.14.cloned.1.call-done = bf16[2048,1536]{1,0:T(8,128)(2,1)} async-done(((bf16[256,1536]{1,0:T(8,128)(2,1)}), bf16[2048,1536]{1,0:T(8,128)(2,1)}) %all-gather.14.cloned.1.call-update) | async-done | bytes 6291472 | tf_op jit(solution)/shard_map/all_gather | solution.py:69
  123.5 5.3 fusion.9
  141.0 6.5 fusion.11
  153.3 5.5 slice.220
  158.8 5.5 slice.224
  164.3 4.1 fusion.30
  168.4 3.3 slice.227
  175.0 3.3 slice.226
  178.4 3.3 slice.230
  226.4 3.4 slice.225
  229.7 3.3 slice.276
  237.6 5.6 slice.219
  249.4 9.0 %pad.69 = f32[384,1536]{1,0:T(8,128)} pad(f32[192,1536]{1,0:T(8,128)} %add.203, f32[]{:T(128)} %constant.7.clone.1), padding=1_0_1x0_0_0 | pad | bytes 3538948 | tf_op jit(solution)/shard_map/pad | solution.py:102
  260.5 5.0 pad.68
  265.5 8.1 %multiply_convert_fusion.1 = bf16[384,2048]{1,0:T(8,128)(2,1)} fusion(bf16[1536,2048]{1,0:T(8,128)(2,1)} %all-gather.16.cloned.1.call-done, f32[2048]{0:T(1024)S(1)} %bitcast.22, f32[384,1536]{1,0:T(8,128)} %pad.68, f32[384,1536]{1,0:T(8,128)} %pad.69), kind=kOutput, calls=%fused_computation.15 | convolution fusion | flops 2418671616 | bytes 12591104 | tf_op jit(solution)/shard_map/dot_general | solution.py:39
  273.7 7.3 reduce-scatter.3.cloned.1.call-done
  290.9 20.9 %all-gather.3 = bf16[8,1,256]{2,1,0:T(2,128)(2,1)S(1)} all-gather(bf16[1,1,256]{2,1,0:T(2,128)(2,1)S(1)} %reshape.55), channel_id=3, replica_groups=mesh['rep'=2,'fs'=8,'tp'=2] {'fs'}, dimensions={0}, use_global_device_ids=true | all-gather | bytes 4608 | tf_op jit(solution)/shard_map/all_gather | solution.py:133
  313.7 134.7 %all-gather.20.cloned.1.call-done = bf16[2048,2560]{1,0:T(8,128)(2,1)} async-done(((bf16[256,2560]{1,0:T(8,128)(2,1)}), bf16[2048,2560]{1,0:T(8,128)(2,1)}) %all-gather.20.cloned.1.call-update) | async-done | bytes 10485776 | tf_op jit(solution)/shard_map/all_gather | solution.py:119
  448.4 10.6 %convolution_multiply_fusion.1 = f32[384,2560]{1,0:T(8,128)} fusion(bf16[2048,2560]{1,0:T(8,128)(2,1)} %all-gather.20.cloned.1.call-done, f32[2560]{0:T(1024)S(1)} %copy-done.30, bf16[384,2048]{1,0:T(8,128)(2,1)} %all-gather.18.cloned.1.call-done, f32[2048]{0:T(1024)S(1)} %copy-done.34, f32[384]{0:T(512)S(1)} %add_rsqrt_fusion), kind=kOutput, calls=%fused_computation.2 | convolution fusion | flops 4030660608 | bytes 16010752 | tf_op jit(solution)/shard_map/dot_general | solution.py:34
  459.0 140.3 %all-gather.22.cloned.1.call-done = bf16[2048,2560]{1,0:T(8,128)(2,1)} async-done(((bf16[256,2560]{1,0:T(8,128)(2,1)}), bf16[2048,2560]{1,0:T(8,128)(2,1)}) %all-gather.22.cloned.1.call-update) | async-done | bytes 10485776 | tf_op jit(solution)/shard_map/all_gather | solution.py:123
  599.3 150.8 %all-gather.24.cloned.1.call-done = bf16[2560,2048]{1,0:T(8,128)(2,1)} async-done(((bf16[2560,256]{1,0:T(8,128)(2,1)}), bf16[2560,2048]{1,0:T(8,128)(2,1)}) %all-gather.24.cloned.1.call-update) | async-done | bytes 10485776 | tf_op jit(solution)/shard_map/all_gather | solution.py:132
  750.1 17.9 %multiply_convert_fusion = bf16[384,2048]{1,0:T(8,128)(2,1)} fusion(bf16[2560,2048]{1,0:T(8,128)(2,1)} %all-gather.24.cloned.1.call-done, f32[2048]{0:T(1024)S(1)} %bitcast.23, bf16[2048,2560]{1,0:T(8,128)(2,1)} %all-gather.22.cloned.1.call-done, f32[384,2560]{1,0:T(8,128)} %convolution_multiply_fusion.1, f32[2560]{0:T(1024)S(1)} %copy-done.31, ...), kind=kOutput, calls=%fused_computation.14 | convolution fusion | flops 8064663552 | bytes 28077568 | tf_op jit(solution)/shard_map/dot_general | solution.py:39
  768.0 7.3 reduce-scatter.5.cloned.1.call-done
  (203 shorter events, 99.3 us)
Async XLA Ops:
  6.5 126.2 %copy-start = (bf16[12,128,128]{2,1,0:T(8,128)(2,1)S(1)}, bf16[12,128,128]{2,1,0:T(8,128)(2,1)}, u32[]{:S(2)}) copy-start(bf16[12,128,128]{2,1,0:T(8,128)(2,1)} %param.23) | copy-start | bytes 1179652
  6.5 27.4 %all-gather.12.cloned.1.call-start = ((), (), s32[]{:S(2)}) async-start(), calls=%async_computation.2 | async-start | bytes 2359296 | tf_op jit(solution)/shard_map/all_gather | solution.py:17
  7.3 116.3 %all-gather.14.cloned.1.call-start = ((), (), s32[]{:S(2)}) async-start(), calls=%async_computation.3 | async-start | bytes 7077888 | tf_op jit(solution)/shard_map/all_gather | solution.py:69
  9.7 113.8 %copy-start.32 = (f32[2048]{0:T(1024)S(1)}, f32[2048]{0:T(1024)}, u32[]{:S(2)}) copy-start(f32[2048]{0:T(1024)} %param.19) | copy-start | bytes 24580
  9.8 113.8 %copy-start.33 = (f32[1536]{0:T(1024)S(1)}, f32[1536]{0:T(1024)}, u32[]{:S(2)}) copy-start(f32[1536]{0:T(1024)} %param.21) | copy-start | bytes 18436
  9.8 255.7 %all-gather.16.cloned.1.call-start = ((), (), s32[]{:S(2)}) async-start(), calls=%async_computation.4 | async-start | bytes 7077888 | tf_op jit(solution)/shard_map/all_gather | solution.py:108
  10.8 270.2 %reduce-scatter.3.cloned.1.call-start = ((), (), s32[]{:S(2)}) async-start(), calls=%async_computation.5 | async-start | bytes 2359296 | tf_op jit(solution)/shard_map/reduce_scatter | solution.py:22
  234.4 9.4 %copy-start.17 = (f32[3,1536]{1,0:T(4,128)S(1)}, f32[3,1536]{1,0:T(4,128)}, u32[]{:S(2)}) copy-start(f32[3,1536]{1,0:T(4,128)} %slice.260) | copy-start | bytes 55300
  234.4 9.5 %copy-start.18 = (f32[2,1536]{1,0:T(2,128)S(1)}, f32[2,1536]{1,0:T(2,128)}, u32[]{:S(2)}) copy-start(f32[2,1536]{1,0:T(2,128)} %slice.266) | copy-start | bytes 36868
  234.5 9.6 %copy-start.23 = (f32[1,1536]{1,0:T(1,128)S(1)}, f32[1,1536]{1,0:T(1,128)}, u32[]{:S(2)}) copy-start(f32[1,1536]{1,0:T(1,128)} %slice.285) | copy-start | bytes 18436
  234.5 9.6 %copy-start.13 = (f32[5,1536]{1,0:T(8,128)S(1)}, f32[5,1536]{1,0:T(8,128)}, u32[]{:S(2)}) copy-start(f32[5,1536]{1,0:T(8,128)} %slice.268) | copy-start | bytes 92164
  234.5 9.6 %copy-start.22 = (f32[1,1536]{1,0:T(1,128)S(1)}, f32[1,1536]{1,0:T(1,128)}, u32[]{:S(2)}) copy-start(f32[1,1536]{1,0:T(1,128)} %slice.284) | copy-start | bytes 18436
  265.5 15.5 %copy-start.3 = (bf16[384,1024]{1,0:T(8,128)(2,1)S(1)}, bf16[384,1024]{1,0:T(8,128)(2,1)}, u32[]{:S(2)}) copy-start(bf16[384,1024]{1,0:T(8,128)(2,1)} %param.18) | copy-start | bytes 2359300
  273.7 38.2 %all-gather.18.cloned.1.call-start = ((), (), s32[]{:S(2)}) async-start(), calls=%async_computation.6 | async-start | bytes 2359296 | tf_op jit(solution)/shard_map/all_gather | solution.py:17
  283.4 165.0 %all-gather.20.cloned.1.call-start = ((), (), s32[]{:S(2)}) async-start(), calls=%async_computation.7 | async-start | bytes 11796480 | tf_op jit(solution)/shard_map/all_gather | solution.py:119
  286.5 312.7 %all-gather.22.cloned.1.call-start = ((), (), s32[]{:S(2)}) async-start(), calls=%async_computation.8 | async-start | bytes 11796480 | tf_op jit(solution)/shard_map/all_gather | solution.py:123
  287.8 462.2 %all-gather.24.cloned.1.call-start = ((), (), s32[]{:S(2)}) async-start(), calls=%async_computation.9 | async-start | bytes 11796480 | tf_op jit(solution)/shard_map/all_gather | solution.py:132
  290.8 157.5 %copy-start.30 = (f32[2560]{0:T(1024)S(1)}, f32[2560]{0:T(1024)}, u32[]{:S(2)}) copy-start(f32[2560]{0:T(1024)} %param.31) | copy-start | bytes 30724
  290.8 157.5 %copy-start.34 = (f32[2048]{0:T(1024)S(1)}, f32[2048]{0:T(1024)}, u32[]{:S(2)}) copy-start(f32[2048]{0:T(1024)} %param.29) | copy-start | bytes 24580
  290.9 484.4 %reduce-scatter.5.cloned.1.call-start = ((), (), s32[]{:S(2)}) async-start(), calls=%async_computation.10 | async-start | bytes 2359296 | tf_op jit(solution)/shard_map/reduce_scatter | solution.py:22
  313.7 436.4 %copy-start.8 = (bf16[384,2048]{1,0:T(8,128)(2,1)S(1)}, bf16[384,2048]{1,0:T(8,128)(2,1)}, u32[]{:S(2)}) copy-start(bf16[384,2048]{1,0:T(8,128)(2,1)} %all-gather.18.cloned.1.call-done) | copy-start | bytes 4718596
  313.7 436.4 %copy-start.31 = (f32[2560]{0:T(1024)S(1)}, f32[2560]{0:T(1024)}, u32[]{:S(2)}) copy-start(f32[2560]{0:T(1024)} %param.33) | copy-start | bytes 30724
  750.1 25.2 %copy-start.2 = (bf16[384,1024]{1,0:T(8,128)(2,1)S(1)}, bf16[384,1024]{1,0:T(8,128)(2,1)}, u32[]{:S(2)}) copy-start(bf16[384,1024]{1,0:T(8,128)(2,1)} %add_convert_fusion.2) | copy-start | bytes 2359300
  750.1 27.5 %copy-start.1 = (bf16[12,128,128]{2,1,0:T(8,128)(2,1)S(1)}, bf16[12,128,128]{2,1,0:T(8,128)(2,1)}, u32[]{:S(2)}) copy-start(bf16[12,128,128]{2,1,0:T(8,128)(2,1)} %param.23) | copy-start | bytes 1179652
  (22 other events, 76.1 us)
Sparse Core Ops, SparseCore 0:
  8.9 12.5 all-gather.11
  23.6 99.8 all-gather.13
  125.6 97.6 all-gather.15
  273.8 7.1 reduce-scatter.2
  283.5 11.0 all-gather.17
  296.6 151.6 all-gather.19
  450.6 148.6 all-gather.21
  601.3 148.6 all-gather.23
  768.1 7.0 reduce-scatter.4
where the time goes:
time: 786 us; the launch traced here: 784 us
  waiting for transfers between devices  529 us (67%)
  local copies, waits for them, and re-layouts  104 us (13%)
  other arithmetic  48 us (6%)
  matrix products  46.2 us (6%)
  blocking collectives  43.2 us (5%)
  between operations  13.9 us (2%)
    all_gather x1, waiting for transfers between devices, body(): lax.all_gather(feedforward_down_weight.astype(jnp.bfloat16), 'fs', axis=1...  151 us
    all_gather x1, waiting for transfers between devices, body(): lax.all_gather(feedforward_up_weight.astype(jnp.bfloat16), 'fs', axis=0,...  140 us
    all_gather x1, waiting for transfers between devices, body(): lax.all_gather(feedforward_gate_weight.astype(jnp.bfloat16), 'fs', axis=0...  135 us
    all_gather x1, waiting for transfers between devices, body(): lax.all_gather(recurrent_input_weight.astype(jnp.bfloat16), 'fs', axis=0,...  87.7 us
    slice x49, local copies, waits for them, and re-layouts, body(): _, state = lax.associative_scan(combine_pairs, (decay, drive), axis=0)  82.4 us
    dot_general x2, matrix products, place_columns(): jnp.dot(left_rows, weight_piece, preferred_element_type=jnp.float32)  26.1 us
    all_gather x1, blocking collectives, body(): lax.all_gather(mixing_output_scale.reshape(1, -1).astype(jnp.bfloat16), '...  22.3 us
    all_gather x1, blocking collectives, body(): lax.all_gather(feedforward_down_scale.reshape(1, -1).astype(jnp.bfloat16)...  20.9 us
  transfers between devices with their start and end apart: 9, of which 6 were waited for; matrix products, arithmetic and copies ran while one was open for 21% of the time, Pallas kernels for 0%

commit v1 on v0

--- a/solution.py
+++ b/solution.py
@@ -66,7 +66,15 @@
     width_dev = recurrent_input_weight.shape[1]
     rec_sum = add_one(
         normed,
-        lax.all_gather(recurrent_input_weight.astype(jnp.bfloat16), "fs", axis=0, tiled=True),
+        jnp.concatenate(
+            lax.all_to_all(
+                jnp.stack([recurrent_input_weight.astype(jnp.bfloat16)] * lax.axis_size("fs")),
+                "fs",
+                0,
+                0,
+            ),
+            axis=0,
+        ),
     )
     rec_input = (rec_sum * recurrent_input_scale).astype(jnp.bfloat16)
     rec_f32 = rec_input.astype(jnp.float32)

time: 786 us -> 905 us (1.15)
  blocking collectives: 43.2 us -> 161 us
    all_gather x1, blocking collectives: 22.3 us -> 140 us  [body(): lax.all_gather(mixing_output_scale.reshape(1, -1).astype(jnp.bfloat16), '...]
    all_gather x1 -> x0, waiting for transfers between devices: 87.7 us -> none  [body(): lax.all_gather(recurrent_input_weight.astype(jnp.bfloat16), 'fs', axis=0,...]
    all_to_all x0 -> x1, waiting for transfers between devices: none -> 67.2 us  [body(): lax.all_to_all(jnp.stack([recurrent_input_weight.astype(jnp.bfloat16)] *...]
    reduce_scatter x2, waiting for transfers between devices: 14.6 us -> 26 us  [share_sums(): lax.psum_scatter(terms.astype(jnp.bfloat16), 'tp', scatter_dimension=1, t...]
  transfers between devices with their start and end apart: 9 -> 9, of which waited for: 6 -> 6; matrix products, arithmetic and copies ran while one was open for 21% -> 18% of each run, Pallas kernels for 0% -> 0%
where the time goes in v1:
time: 905 us; the launch traced here: 903 us
  waiting for transfers between devices  520 us (57%)
  blocking collectives  161 us (18%)
  local copies, waits for them, and re-layouts  107 us (12%)
  other arithmetic  47 us (5%)
  matrix products  46.1 us (5%)
  between operations  14.2 us (2%)
    all_gather x1, waiting for transfers between devices, body(): lax.all_gather(feedforward_down_weight.astype(jnp.bfloat16), 'fs', axis=1...  151 us
    all_gather x1, blocking collectives, body(): lax.all_gather(mixing_output_scale.reshape(1, -1).astype(jnp.bfloat16), '...  140 us
    all_gather x1, waiting for transfers between devices, body(): lax.all_gather(feedforward_up_weight.astype(jnp.bfloat16), 'fs', axis=0,...  140 us
    all_gather x1, waiting for transfers between devices, body(): lax.all_gather(feedforward_gate_weight.astype(jnp.bfloat16), 'fs', axis=0...  135 us
    slice x49, local copies, waits for them, and re-layouts, body(): _, state = lax.associative_scan(combine_pairs, (decay, drive), axis=0)  82.4 us
    all_to_all x1, waiting for transfers between devices, body(): lax.all_to_all(jnp.stack([recurrent_input_weight.astype(jnp.bfloat16)] *...  67.2 us
    dot_general x2, matrix products, place_columns(): jnp.dot(left_rows, weight_piece, preferred_element_type=jnp.float32)  26.1 us
    reduce_scatter x2, waiting for transfers between devices, share_sums(): lax.psum_scatter(terms.astype(jnp.bfloat16), 'tp', scatter_dimension=1, t...  26 us
  transfers between devices with their start and end apart: 9, of which 6 were waited for; matrix products, arithmetic and copies ran while one was open for 18% of the time, Pallas kernels for 0%

profile of v1, /device:TPU:0, one launch (start us, length us, event | category | flops | bytes accessed | tf_op | source)
XLA Modules:
  0.0 903.0 jit_solution(7860505882854231391)
XLA Ops:
  11.2 7.4 all-to-all-start
  20.6 140.4 %all-gather.2 = bf16[8,1,256]{2,1,0:T(2,128)(2,1)S(1)} all-gather(bf16[1,1,256]{2,1,0:T(2,128)(2,1)S(1)} %reshape.59), channel_id=2, replica_groups=mesh['rep'=2,'fs'=8,'tp'=2] {'fs'}, dimensions={0}, use_global_device_ids=true | all-gather | bytes 4608 | tf_op jit(solution)/shard_map/all_gather | solution.py:117
  163.6 67.2 %all-to-all-done = bf16[8,256,1536]{2,1,0:T(8,128)(2,1)} async-done(((bf16[8,256,1536]{2,1,0:T(8,128)(2,1)}), bf16[8,256,1536]{2,1,0:T(8,128)(2,1)}, u32[]{:S(2)}, u32[]{:S(2)}) %all-to-all-start) | async-done | bytes 6291488 | tf_op jit(solution)/shard_map/all_to_all | solution.py:70
  230.8 5.3 fusion.9
  248.2 6.5 fusion.11
  260.5 5.5 slice.220
  266.0 5.5 slice.224
  271.5 4.1 fusion.30
  275.6 3.3 slice.227
  285.5 3.3 slice.230
  333.5 3.4 slice.225
  336.9 3.3 slice.276
  344.8 5.6 slice.219
  356.6 9.0 %pad.69 = f32[384,1536]{1,0:T(8,128)} pad(f32[192,1536]{1,0:T(8,128)} %add.203, f32[]{:T(128)} %constant.7.clone.1), padding=1_0_1x0_0_0 | pad | bytes 3538948 | tf_op jit(solution)/shard_map/pad | solution.py:110
  367.8 5.0 pad.68
  372.8 8.1 multiply_convert_fusion.1
  381.0 18.7 %reduce-scatter.3.cloned.1.call-done = bf16[384,1024]{1,0:T(8,128)(2,1)} async-done(((bf16[384,2048]{1,0:T(8,128)(2,1)}), bf16[384,1024]{1,0:T(8,128)(2,1)}) %reduce-scatter.3.cloned.1.call-update) | async-done | bytes 786448 | tf_op jit(solution)/shard_map/reduce_scatter | solution.py:22
  409.7 20.9 %all-gather.3 = bf16[8,1,256]{2,1,0:T(2,128)(2,1)S(1)} all-gather(bf16[1,1,256]{2,1,0:T(2,128)(2,1)S(1)} %reshape.61), channel_id=3, replica_groups=mesh['rep'=2,'fs'=8,'tp'=2] {'fs'}, dimensions={0}, use_global_device_ids=true | all-gather | bytes 4608 | tf_op jit(solution)/shard_map/all_gather | solution.py:141
  432.5 134.6 %all-gather.17.cloned.1.call-done = bf16[2048,2560]{1,0:T(8,128)(2,1)} async-done(((bf16[256,2560]{1,0:T(8,128)(2,1)}), bf16[2048,2560]{1,0:T(8,128)(2,1)}) %all-gather.17.cloned.1.call-update) | async-done | bytes 10485776 | tf_op jit(solution)/shard_map/all_gather | solution.py:127
  567.1 10.6 %convolution_multiply_fusion.1 = f32[384,2560]{1,0:T(8,128)} fusion(bf16[2048,2560]{1,0:T(8,128)(2,1)} %all-gather.17.cloned.1.call-done, f32[2560]{0:T(1024)S(1)} %copy-done.30, bf16[384,2048]{1,0:T(8,128)(2,1)} %all-gather.15.cloned.1.call-done, f32[2048]{0:T(1024)S(1)} %copy-done.34, f32[384]{0:T(512)S(1)} %add_rsqrt_fusion), kind=kOutput, calls=%fused_computation.2 | convolution fusion | flops 4030660608 | bytes 16010752 | tf_op jit(solution)/shard_map/dot_general | solution.py:34
  577.7 140.2 %all-gather.19.cloned.1.call-done = bf16[2048,2560]{1,0:T(8,128)(2,1)} async-done(((bf16[256,2560]{1,0:T(8,128)(2,1)}), bf16[2048,2560]{1,0:T(8,128)(2,1)}) %all-gather.19.cloned.1.call-update) | async-done | bytes 10485776 | tf_op jit(solution)/shard_map/all_gather | solution.py:131
  717.9 150.8 %all-gather.21.cloned.1.call-done = bf16[2560,2048]{1,0:T(8,128)(2,1)} async-done(((bf16[2560,256]{1,0:T(8,128)(2,1)}), bf16[2560,2048]{1,0:T(8,128)(2,1)}) %all-gather.21.cloned.1.call-update) | async-done | bytes 10485776 | tf_op jit(solution)/shard_map/all_gather | solution.py:140
  868.6 17.9 %multiply_convert_fusion = bf16[384,2048]{1,0:T(8,128)(2,1)} fusion(bf16[2560,2048]{1,0:T(8,128)(2,1)} %all-gather.21.cloned.1.call-done, f32[2048]{0:T(1024)S(1)} %bitcast.24, bf16[2048,2560]{1,0:T(8,128)(2,1)} %all-gather.19.cloned.1.call-done, f32[384,2560]{1,0:T(8,128)} %convolution_multiply_fusion.1, f32[2560]{0:T(1024)S(1)} %copy-done.31, ...), kind=kOutput, calls=%fused_computation.14 | convolution fusion | flops 8064663552 | bytes 28077568 | tf_op jit(solution)/shard_map/dot_general | solution.py:39
  886.6 7.3 reduce-scatter.5.cloned.1.call-done
  (203 shorter events, 104.8 us)
Async XLA Ops:
  6.5 233.4 %copy-start = (bf16[12,128,128]{2,1,0:T(8,128)(2,1)S(1)}, bf16[12,128,128]{2,1,0:T(8,128)(2,1)}, u32[]{:S(2)}) copy-start(bf16[12,128,128]{2,1,0:T(8,128)(2,1)} %param.23) | copy-start | bytes 1179652
  11.2 219.5 %all-to-all-start = ((bf16[8,256,1536]{2,1,0:T(8,128)(2,1)}), bf16[8,256,1536]{2,1,0:T(8,128)(2,1)}, u32[]{:S(2)}, u32[]{:S(2)}) async-start(bf16[8,256,1536]{2,1,0:T(8,128)(2,1)} %stack.2), calls=%async_computation | async-start | bytes 12582912 | tf_op jit(solution)/shard_map/all_to_all | solution.py:70
  18.7 143.0 %copy-start.21 = (f32[4,1536]{1,0:T(4,128)S(1)}, f32[4,1536]{1,0:T(4,128)}, u32[]{:S(2)}) copy-start(f32[4,1536]{1,0:T(4,128)} %param.22) | copy-start | bytes 73732
  18.7 143.0 %copy-start.26 = (f32[1536]{0:T(1024)S(1)}, f32[1536]{0:T(1024)}, u32[]{:S(2)}) copy-start(f32[1536]{0:T(1024)} %param.25) | copy-start | bytes 18436
  18.7 143.1 %all-gather.11.cloned.1.call-start = ((), (), s32[]{:S(2)}) async-start(), calls=%async_computation.3 | async-start | bytes 2359296 | tf_op jit(solution)/shard_map/all_gather | solution.py:17
  19.4 211.3 %copy-start.32 = (f32[2048]{0:T(1024)S(1)}, f32[2048]{0:T(1024)}, u32[]{:S(2)}) copy-start(f32[2048]{0:T(1024)} %param.19) | copy-start | bytes 24580
  19.4 211.3 %copy-start.33 = (f32[1536]{0:T(1024)S(1)}, f32[1536]{0:T(1024)}, u32[]{:S(2)}) copy-start(f32[1536]{0:T(1024)} %param.21) | copy-start | bytes 18436
  19.4 353.3 %all-gather.13.cloned.1.call-start = ((), (), s32[]{:S(2)}) async-start(), calls=%async_computation.4 | async-start | bytes 7077888 | tf_op jit(solution)/shard_map/all_gather | solution.py:116
  20.5 379.3 %reduce-scatter.3.cloned.1.call-start = ((), (), s32[]{:S(2)}) async-start(), calls=%async_computation.5 | async-start | bytes 2359296 | tf_op jit(solution)/shard_map/reduce_scatter | solution.py:22
  341.7 9.6 %copy-start.23 = (f32[1,1536]{1,0:T(1,128)S(1)}, f32[1,1536]{1,0:T(1,128)}, u32[]{:S(2)}) copy-start(f32[1,1536]{1,0:T(1,128)} %slice.285) | copy-start | bytes 18436
  341.7 9.6 %copy-start.13 = (f32[5,1536]{1,0:T(8,128)S(1)}, f32[5,1536]{1,0:T(8,128)}, u32[]{:S(2)}) copy-start(f32[5,1536]{1,0:T(8,128)} %slice.268) | copy-start | bytes 92164
  341.7 9.7 %copy-start.22 = (f32[1,1536]{1,0:T(1,128)S(1)}, f32[1,1536]{1,0:T(1,128)}, u32[]{:S(2)}) copy-start(f32[1,1536]{1,0:T(1,128)} %slice.284) | copy-start | bytes 18436
  372.8 27.0 %copy-start.3 = (bf16[384,1024]{1,0:T(8,128)(2,1)S(1)}, bf16[384,1024]{1,0:T(8,128)(2,1)}, u32[]{:S(2)}) copy-start(bf16[384,1024]{1,0:T(8,128)(2,1)} %param.18) | copy-start | bytes 2359300
  381.0 49.7 %all-gather.15.cloned.1.call-start = ((), (), s32[]{:S(2)}) async-start(), calls=%async_computation.6 | async-start | bytes 2359296 | tf_op jit(solution)/shard_map/all_gather | solution.py:17
  402.1 165.0 %all-gather.17.cloned.1.call-start = ((), (), s32[]{:S(2)}) async-start(), calls=%async_computation.7 | async-start | bytes 11796480 | tf_op jit(solution)/shard_map/all_gather | solution.py:127
  405.3 312.6 %all-gather.19.cloned.1.call-start = ((), (), s32[]{:S(2)}) async-start(), calls=%async_computation.8 | async-start | bytes 11796480 | tf_op jit(solution)/shard_map/all_gather | solution.py:131
  406.6 462.0 %all-gather.21.cloned.1.call-start = ((), (), s32[]{:S(2)}) async-start(), calls=%async_computation.9 | async-start | bytes 11796480 | tf_op jit(solution)/shard_map/all_gather | solution.py:140
  409.6 157.5 %copy-start.30 = (f32[2560]{0:T(1024)S(1)}, f32[2560]{0:T(1024)}, u32[]{:S(2)}) copy-start(f32[2560]{0:T(1024)} %param.31) | copy-start | bytes 30724
  409.6 157.5 %copy-start.34 = (f32[2048]{0:T(1024)S(1)}, f32[2048]{0:T(1024)}, u32[]{:S(2)}) copy-start(f32[2048]{0:T(1024)} %param.29) | copy-start | bytes 24580
  409.6 484.3 %reduce-scatter.5.cloned.1.call-start = ((), (), s32[]{:S(2)}) async-start(), calls=%async_computation.10 | async-start | bytes 2359296 | tf_op jit(solution)/shard_map/reduce_scatter | solution.py:22
  432.4 436.2 %copy-start.8 = (bf16[384,2048]{1,0:T(8,128)(2,1)S(1)}, bf16[384,2048]{1,0:T(8,128)(2,1)}, u32[]{:S(2)}) copy-start(bf16[384,2048]{1,0:T(8,128)(2,1)} %all-gather.15.cloned.1.call-done) | copy-start | bytes 4718596
  432.5 436.2 %copy-start.31 = (f32[2560]{0:T(1024)S(1)}, f32[2560]{0:T(1024)}, u32[]{:S(2)}) copy-start(f32[2560]{0:T(1024)} %param.33) | copy-start | bytes 30724
  868.6 25.2 %copy-start.2 = (bf16[384,1024]{1,0:T(8,128)(2,1)S(1)}, bf16[384,1024]{1,0:T(8,128)(2,1)}, u32[]{:S(2)}) copy-start(bf16[384,1024]{1,0:T(8,128)(2,1)} %add_convert_fusion.2) | copy-start | bytes 2359300
  868.6 27.6 %copy-start.1 = (bf16[12,128,128]{2,1,0:T(8,128)(2,1)S(1)}, bf16[12,128,128]{2,1,0:T(8,128)(2,1)}, u32[]{:S(2)}) copy-start(bf16[12,128,128]{2,1,0:T(8,128)(2,1)} %param.23) | copy-start | bytes 1179652
  (22 other events, 98.4 us)
Sparse Core Ops, SparseCore 0:
  21.0 11.1 all-gather.10
  34.3 198.7 all-gather.12
  381.1 18.6 reduce-scatter.2
  402.2 11.0 all-gather.14
  415.4 151.6 all-gather.16
  569.1 148.6 all-gather.18
  719.9 148.6 all-gather.20
  886.7 7.1 reduce-scatter.4
